TPU v7x, 256 devices: a whole 4x4x8 slice. The times are simulated.
256 devices in a mesh: sp: 32 (over z, x), tp: 8 (over y, core).
Axes of the slice: x: 4, y: 4, z: 8, core: 2. Of those that a mesh axis runs over, the one named last changes fastest.
Arguments:
- tokens: bfloat16 [16384, 2048], P(('sp', 'tp')), may hold values from -6 to 6
- input_gain: bfloat16 [2048], replicated, may hold values from 0.099609375 to 1.8984375
- weight_query: bfloat16 [2048, 1024], P(None, 'tp'), may hold values from -0.125 to 0.125
- weight_key: bfloat16 [2048, 1024], P(None, 'tp'), may hold values from -0.125 to 0.125
- weight_value: bfloat16 [2048, 2048], P(None, 'tp'), may hold values from -8 to 8
- weight_outgate: bfloat16 [2048, 2048], P(None, 'tp'), may hold values from -0.125 to 0.125
- weight_ingate: bfloat16 [2048, 8], replicated, may hold values from -0.125 to 0.125
- weight_forget: bfloat16 [2048, 8], replicated, may hold values from -0.125 to 0.125
- forget_shift: float32 [16384, 8], P('sp', 'tp'), may hold values from 0 to 20
- mem_gain: bfloat16 [2048], replicated, may hold values from 0.099609375 to 1.8984375
- query_down_weight: bfloat16 [2048, 768], P(None, 'tp'), may hold values from -0.125 to 0.125
- latent_down_weight: bfloat16 [2048, 512], P(None, 'tp'), may hold values from -0.125 to 0.125
- down_rotary: bfloat16 [2048, 64], replicated, may hold values from -0.125 to 0.125
- query_gain: float32 [768], replicated, may hold values from 0.15 to 12
- latent_gain: float32 [512], replicated, may hold values from 0.15 to 12
- query_up_weight: bfloat16 [768, 1536], P(None, 'tp'), may hold values from -0.4375 to 0.4375
- key_up_weight: bfloat16 [512, 1024], P(None, 'tp'), may hold values from -0.25 to 0.25
- value_up_weight: bfloat16 [512, 1024], P(None, 'tp'), may hold values from -0.25 to 0.25
- out_memory: bfloat16 [2048, 2048], P('tp'), may hold values from -0.5 to 0.5
- out_attend: bfloat16 [1024, 2048], P('tp'), may hold values from -0.75 to 0.75
Outputs:
- mixed: bfloat16 [16384, 2048], P(('sp', 'tp'))
All inputs are finite; a program needn't handle non-finite values.
Results may differ from a plain program's by a relative error of at most 0.04.
The roundings to bfloat16 on the way count: a program that leaves them out, or rounds other values in their place, can miss the bound.
Values may be sent and summed in bfloat16 or wider, within the bound.
No kernel may reach another device: no remote copies, remote signals or barrier semaphores. Data moves between devices by JAX's collectives and lax.ppermute only.
A program may use at most 128 MiB of HBM per device.

v0:
```python
import math
import jax
import jax.numpy as jnp
from jax import lax
from jax.sharding import Mesh
from jax.sharding import PartitionSpec as P

MEMORY_HEADS = 8
M_QK = 128
M_V = 256
PLAIN_CHANNELS = 128
ROTARY_CHANNELS = 64
VALUE_CHANNELS = 128
BLOCK = 64
SP = ("sp_0", "sp_1")
SP_TP = ("sp_0", "sp_1", "tp")
SMALL_CONSTANT = 1e-06
SOFTCAP = 15.0
ROTARY_BASE = 10000.0
PRECISE = lax.Precision.HIGHEST
FAR_BELOW = -1e30


def copy_for_each(shard, axis):
    copies = jnp.broadcast_to(shard, (lax.axis_size(axis), *shard.shape))
    return lax.all_to_all(copies, axis, split_axis=0, concat_axis=0, tiled=True)


def laid_out(tiles, dim):
    shape = list(tiles.shape[1:])
    shape[dim] *= tiles.shape[0]
    return jnp.moveaxis(tiles, 0, dim).reshape(shape)


def gather_directly(shard, axis, dim):
    tiles = copy_for_each(shard, axis)
    return laid_out(tiles, dim)


def nothing_yet(shard, identity):
    return jax.tree.map(
        lambda a, e: jnp.broadcast_to(jnp.asarray(e, a.dtype), a.shape), shard, identity
    )


def gathered_once(shard, axis):
    leaves = jax.tree.leaves(shard)
    order = sorted(range(len(leaves)), key=lambda k: -leaves[k].size)
    width = (1, *leaves[order[0]].shape)[-1]
    lines = [
        jnp.pad(leaves[k].reshape(-1), (0, -leaves[k].size % width)).reshape(-1, width)
        for k in order
    ]
    both, at, found = (lax.all_gather(jnp.concatenate(lines), axis), 0, {})
    for k, line in zip(order, lines):
        slab = both[:, at : at + len(line)].reshape(len(both), -1)
        found[k] = slab[:, : leaves[k].size].reshape(-1, *leaves[k].shape)
        at += len(line)
    numbers = iter(range(len(leaves)))
    return jax.tree.map(lambda _: found[next(numbers)], shard)


def entering(shard, axes, combine, identity):
    before = start = nothing_yet(shard, identity)
    running = shard
    for axis in reversed(axes):
        peers, index = (lax.axis_size(axis), lax.axis_index(axis))
        pieces = gathered_once(running, axis)
        inside, running = (start, start)
        for k in range(peers):
            passed = k < index
            running = combine(running, jax.tree.map(lambda part: part[k], pieces))
            inside = jax.tree.map(lambda new, old: jnp.where(passed, new, old), running, inside)
        before = combine(inside, before)
    return before


def side_by_side(arrays, axis, dim, along):
    ends, at = ([], 0)
    for a in arrays[:-1]:
        at += a.shape[along]
        ends.append(at)
    both = jnp.concatenate(arrays, axis=along)
    return tuple(jnp.split(lax.all_gather(both, axis, axis=dim, tiled=True), ends, axis=along))


def in_blocks(shard, dim, peers):
    shape = shard.shape
    tiles = shard.reshape(*shape[:dim], peers, shape[dim] // peers, *shape[dim + 1 :])
    return jnp.moveaxis(tiles, dim, 0)


def sum_at_owner(shard, axis, dim):
    tiles = in_blocks(shard, dim, lax.axis_size(axis))
    arrived = lax.all_to_all(tiles, axis, split_axis=0, concat_axis=0, tiled=True)
    return arrived.astype(jnp.float32).sum(axis=0)


def rms_scale(values, gain):
    widened = values.astype(jnp.float32)
    return (
        widened
        * lax.rsqrt(jnp.mean(widened * widened, axis=-1, keepdims=True) + SMALL_CONSTANT)
        * gain.astype(jnp.float32)
    )


def rotate(values, positions):
    halfway = values.shape[-1] // 2
    inverse = jnp.power(ROTARY_BASE, -jnp.arange(halfway, dtype=jnp.float32) / halfway)
    angles = positions.astype(jnp.float32)[:, None] * inverse
    cosine = jnp.cos(angles)
    sine_part = jnp.sin(angles)
    if values.ndim == 3:
        cosine = cosine[:, None, :]
        sine_part = sine_part[:, None, :]
    widened = values.astype(jnp.float32)
    first = widened[..., :halfway]
    second = widened[..., halfway:]
    turned = jnp.concatenate(
        [first * cosine - second * sine_part, second * cosine + first * sine_part], axis=-1
    )
    return turned.astype(jnp.bfloat16)


def update_state(carried, key_rows, value_rows, input_gate, cumulative):
    matrix, normal, stabilizer = carried
    last_total = cumulative[:, -1]
    weight_log = last_total[:, None] - cumulative + input_gate
    new_max = jnp.maximum(last_total + stabilizer, jnp.max(weight_log, axis=-1))
    weights = jnp.exp(weight_log - new_max[:, None])
    decay = jnp.exp(last_total + stabilizer - new_max)
    matrix = decay[:, None, None] * matrix + jnp.einsum(
        "hsv,hsd->hvd", weights[:, :, None] * value_rows, key_rows, precision=PRECISE
    )
    normal = decay[:, None] * normal + jnp.einsum(
        "hs,hsd->hd", weights, key_rows, precision=PRECISE
    )
    return (matrix, normal, new_max)


def block_step(carried, inputs):
    query_rows, key_rows, value_rows, input_gate, log_forget = inputs
    matrix, normal, stabilizer = carried
    cumulative = jnp.cumsum(log_forget, axis=-1)
    block_len = log_forget.shape[-1]
    causal = jnp.tril(jnp.ones((block_len, block_len), dtype=bool))
    pair_log = cumulative[:, :, None] - cumulative[:, None, :] + input_gate[:, None, :]
    pair_log = jnp.where(causal, pair_log, -jnp.inf)
    carried_log = cumulative + stabilizer[:, None]
    row_max = jnp.maximum(carried_log, jnp.max(pair_log, axis=-1))
    within = jnp.exp(pair_log - row_max[:, :, None])
    across = jnp.exp(carried_log - row_max)
    affinity = jnp.einsum("hjd,hsd->hjs", query_rows, key_rows, precision=PRECISE) * within
    numerator = jnp.einsum("hjs,hsv->hjv", affinity, value_rows, precision=PRECISE)
    numerator = numerator + across[:, :, None] * jnp.einsum(
        "hjd,hvd->hjv", query_rows, matrix, precision=PRECISE
    )
    denominator = jnp.sum(affinity, axis=-1) + across * jnp.einsum(
        "hjd,hd->hj", query_rows, normal, precision=PRECISE
    )
    output = numerator / jnp.maximum(jnp.abs(denominator), jnp.exp(-row_max))[:, :, None]
    return (update_state(carried, key_rows, value_rows, input_gate, cumulative), output)


def summary_step(carried, inputs):
    key_rows, value_rows, input_gate, log_forget = inputs
    return (
        update_state(carried, key_rows, value_rows, input_gate, jnp.cumsum(log_forget, axis=-1)),
        None,
    )


def merge_states(earlier, later):
    decayed = later[3] + earlier[2]
    joined = jnp.maximum(decayed, later[2])
    early_part = jnp.exp(decayed - joined)
    late_part = jnp.exp(later[2] - joined)
    return (
        early_part[:, None, None] * earlier[0] + late_part[:, None, None] * later[0],
        early_part[:, None] * earlier[1] + late_part[:, None] * later[1],
        joined,
        earlier[3] + later[3],
    )


def per_device(
    tokens,
    input_gain,
    weight_query,
    weight_key,
    weight_value,
    weight_outgate,
    weight_ingate,
    weight_forget,
    forget_shift,
    mem_gain,
    query_down_weight,
    latent_down_weight,
    down_rotary,
    query_gain,
    latent_gain,
    query_up_weight,
    key_up_weight,
    value_up_weight,
    out_memory,
    out_attend,
):
    normed = rms_scale(tokens, input_gain).astype(jnp.bfloat16)
    tp_index = lax.axis_index("tp")
    mem_heads = weight_query.shape[1] // M_QK
    att_heads = key_up_weight.shape[1] // PLAIN_CHANNELS
    ingate_cols = lax.dynamic_slice_in_dim(weight_ingate, tp_index * mem_heads, mem_heads, 1)
    forget_cols = lax.dynamic_slice_in_dim(weight_forget, tp_index * mem_heads, mem_heads, 1)
    weight_list = (
        weight_query,
        weight_key,
        weight_value,
        weight_outgate,
        query_down_weight,
        latent_down_weight,
        down_rotary,
        ingate_cols,
        forget_cols,
    )

    def project(portion):
        return jnp.concatenate(
            [
                jnp.dot(portion, weight, preferred_element_type=jnp.float32)
                for weight in weight_list
            ],
            axis=1,
        )

    projected = project(gather_directly(normed, "tp", 0))
    sections = []
    offset = 0
    for weight in weight_list:
        sections.append(projected[:, offset : offset + weight.shape[1]])
        offset = offset + weight.shape[1]
    stored = tuple((section.astype(jnp.bfloat16) for section in sections[:7]))
    mem_query, mem_key, mem_value, mem_outgate, query_latent, keyval_latent, key_raw = (
        lax.optimization_barrier(stored)
    )
    in_gate = SOFTCAP * jnp.tanh(sections[7] / SOFTCAP)
    log_forget = jax.nn.log_sigmoid(SOFTCAP * jnp.tanh((sections[8] + forget_shift) / SOFTCAP))
    length = projected.shape[0]
    positions = lax.axis_index(SP) * length + jnp.arange(length, dtype=jnp.int32)
    query_whole, latent_whole = (
        lax.all_gather(query_latent, "tp", axis=1, tiled=True),
        lax.all_gather(keyval_latent, "tp", axis=1, tiled=True),
    )
    normed_query = rms_scale(query_whole, query_gain).astype(jnp.bfloat16)
    normed_latent = rms_scale(latent_whole, latent_gain).astype(jnp.bfloat16)
    block_count = length // BLOCK

    def to_blocks(array, width):
        return (
            array.astype(jnp.float32)
            .reshape(block_count, BLOCK, mem_heads, width)
            .transpose(0, 2, 1, 3)
        )

    def gate_blocks(array):
        return array.reshape(block_count, BLOCK, mem_heads).transpose(0, 2, 1)

    query_blocks = to_blocks(mem_query, M_QK)
    key_blocks = to_blocks(mem_key, M_QK) * M_QK ** (-0.5)
    value_blocks = to_blocks(mem_value, M_V)
    ingate_blocks = gate_blocks(in_gate)
    forget_blocks = gate_blocks(log_forget)
    empty_state = (
        jnp.zeros((mem_heads, M_V, M_QK), jnp.float32),
        jnp.zeros((mem_heads, M_QK), jnp.float32),
        jnp.full((mem_heads,), FAR_BELOW, jnp.float32),
    )
    local_state, _ = lax.scan(
        summary_step, empty_state, (key_blocks, value_blocks, ingate_blocks, forget_blocks)
    )
    identity = empty_state + (jnp.zeros((mem_heads,), jnp.float32),)
    prefix = entering(
        (local_state[0], local_state[1], local_state[2], jnp.sum(log_forget, axis=0)),
        SP,
        merge_states,
        identity,
    )
    start_max = jnp.maximum(prefix[3], prefix[2])
    rescale = jnp.exp(prefix[2] - start_max)
    initial = (prefix[0] * rescale[:, None, None], prefix[1] * rescale[:, None], start_max)
    _, cell = lax.scan(
        block_step, initial, (query_blocks, key_blocks, value_blocks, ingate_blocks, forget_blocks)
    )
    cell = cell.transpose(0, 2, 1, 3).reshape(length, mem_heads * M_V)
    cell_total = lax.psum(jnp.sum(cell * cell, axis=1), "tp")
    gain_part = lax.dynamic_slice_in_dim(mem_gain, tp_index * mem_heads * M_V, mem_heads * M_V, 0)
    gated = (
        cell
        * lax.rsqrt(cell_total / (MEMORY_HEADS * M_V) + SMALL_CONSTANT)[:, None]
        * gain_part.astype(jnp.float32)
    )
    gated = gated * jax.nn.sigmoid(mem_outgate.astype(jnp.float32))
    gated = gated.astype(jnp.bfloat16)
    query_all = jnp.dot(normed_query, query_up_weight, preferred_element_type=jnp.float32).astype(
        jnp.bfloat16
    )
    query_all = query_all.reshape(length, att_heads, PLAIN_CHANNELS + ROTARY_CHANNELS)
    query_nope = query_all[..., :PLAIN_CHANNELS]
    query_rot = rotate(query_all[..., PLAIN_CHANNELS:], positions)
    key_rot = rotate(key_raw, positions)
    factor = (PLAIN_CHANNELS + ROTARY_CHANNELS) ** (-0.5)

    def attend_block(carried, key_nope, key_rotary, value_rows, key_start):
        row_max, summed, accum = carried
        number = key_nope.shape[0]
        key_pos = key_start + jnp.arange(number, dtype=jnp.int32)
        scores = jnp.einsum(
            "qhd,khd->hqk",
            query_nope,
            key_nope.reshape(number, att_heads, PLAIN_CHANNELS),
            preferred_element_type=jnp.float32,
        )
        scores = (
            scores
            + jnp.einsum("qhd,kd->hqk", query_rot, key_rotary, preferred_element_type=jnp.float32)
        ) * factor
        allowed = key_pos[None, :] <= positions[:, None]
        scores = jnp.where(allowed[None], scores, -jnp.inf)
        new_max = jnp.maximum(row_max, jnp.max(scores, axis=-1))
        probs = jnp.exp(scores - new_max[:, :, None])
        shrink = jnp.exp(row_max - new_max)
        summed = summed * shrink + jnp.sum(probs, axis=-1)
        accum = accum * shrink[:, :, None] + jnp.einsum(
            "hqk,khd->hqd",
            probs.astype(jnp.bfloat16),
            value_rows.reshape(number, att_heads, VALUE_CHANNELS),
            preferred_element_type=jnp.float32,
        )
        return (new_max, summed, accum)

    initial_att = (
        jnp.full((att_heads, length), FAR_BELOW, jnp.float32),
        jnp.zeros((att_heads, length), jnp.float32),
        jnp.zeros((att_heads, length, VALUE_CHANNELS), jnp.float32),
    )
    own_nope = jnp.dot(normed_latent, key_up_weight, preferred_element_type=jnp.float32).astype(
        jnp.bfloat16
    )
    own_values = jnp.dot(normed_latent, value_up_weight, preferred_element_type=jnp.float32).astype(
        jnp.bfloat16
    )
    carried = initial_att
    piece_rows = side_by_side((own_nope, key_rot, own_values), SP, 0, 1)
    number = piece_rows[0].shape[0]
    size = math.gcd(number, 1024)

    def one_block(state, block_number):
        begin = block_number * size
        sub_rows = tuple(
            (lax.dynamic_slice_in_dim(member, begin, size, 0) for member in piece_rows)
        )

        def compute(current):
            key_nope, key_rotary, value_rows = sub_rows
            return attend_block(current, key_nope, key_rotary, value_rows, begin)

        return (
            lax.cond(begin <= positions[length - 1], compute, lambda current: current, state),
            None,
        )

    carried, _ = lax.scan(one_block, carried, jnp.arange(number // size, dtype=jnp.int32))
    attended = (carried[2] / carried[1][:, :, None]).astype(jnp.bfloat16)
    attended = attended.transpose(1, 0, 2).reshape(length, att_heads * VALUE_CHANNELS)
    mixed = sum_at_owner(
        (
            jnp.dot(gated, out_memory, preferred_element_type=jnp.float32)
            + jnp.dot(attended, out_attend, preferred_element_type=jnp.float32)
        ).astype(jnp.bfloat16),
        "tp",
        0,
    )
    return mixed.astype(jnp.bfloat16)


def solution(mesh):
    torus = Mesh(mesh.devices.reshape(8, 4, mesh.shape["tp"]), ("sp_0", "sp_1", "tp"))
    in_specs = (
        P(SP_TP, None),
        P(),
        P(None, "tp"),
        P(None, "tp"),
        P(None, "tp"),
        P(None, "tp"),
        P(),
        P(),
        P(SP, "tp"),
        P(),
        P(None, "tp"),
        P(None, "tp"),
        P(),
        P(),
        P(),
        P(None, "tp"),
        P(None, "tp"),
        P(None, "tp"),
        P("tp", None),
        P("tp", None),
    )
    out_specs = P(SP_TP, None)
    return jax.shard_map(
        per_device, mesh=torus, in_specs=in_specs, out_specs=out_specs, check_vma=False
    )
```

profile of v0, /device:TPU:230, one launch (start us, length us, event | category | flops | bytes accessed | tf_op | source)
XLA Modules:
  0.0 451.5 jit_solution(11439639850587882562)
XLA Ops:
  9.5 1.6 broadcast_in_dim.36
  11.1 4.5 all-to-all-start
  15.7 27.1 %all-to-all-done = bf16[8,64,2048]{2,1,0:T(8,128)(2,1)S(1)} async-done(((bf16[8,64,2048]{2,1,0:T(8,128)(2,1)}), bf16[8,64,2048]{2,1,0:T(8,128)(2,1)S(1)}, u32[]{:S(2)}, u32[]{:S(2)}) %all-to-all-start) | async-done | bytes 2097184 | tf_op jit(solution)/shard_map/all_to_all | solution.py:26
  44.3 2.1 negate_reduce_fusion
  54.4 40.7 %while.47 = (s32[]{:T(128)}, f32[1,256,128]{2,1,0:T(8,128)S(1)}, f32[1,128]{1,0:T(1,128)S(1)}, f32[1]{0:T(128)}, f32[8,1,64]{2,1,0:T(1,128)S(1)}, /*index=5*/f32...) while((s32[]{:T(128)}, f32[1,256,128]{2,1,0:T(8,128)S(1)}, ...), condition=%wide.region_4.5_spmd.clone, body=%wide.region_1.0_spmd.clone.sunk | while | flops 25383812 | bytes 401378 | solution.py:278
  95.1 13.5 %all-gather.2 = f32[4,259,128]{2,1,0:T(8,128)S(1)} all-gather(f32[1,259,128]{2,1,0:T(8,128)S(1)} %maximum_bitcast_fusion), channel_id=2, replica_groups=mesh['sp_0'=8,'sp_1'=4,'tp'=8] {'sp_1'}, dimensions={0}, use_global_device_ids=true | all-gather | bytes 663040 | tf_op jit(solution)/shard_map/all_gather | solution.py:54
  120.6 13.1 %all_gather.25 = bf16[512,512]{0,1:T(8,128)(2,1)S(1)} all-gather(bf16[512,64]{0,1:T(8,128)(2,1)S(1)} %copy-done.8), channel_id=1, replica_groups=mesh['sp_0'=8,'sp_1'=4,'tp'=8] {'tp'}, dimensions={1}, use_global_device_ids=true | all-gather | bytes 589824 | tf_op jit(solution)/shard_map/all_gather | solution.py:252
  138.0 13.4 %all_gather.27 = bf16[512,768]{0,1:T(8,128)(2,1)S(1)} all-gather(bf16[512,96]{0,1:T(8,128)(2,1)S(1)} %convolution_convert_fusion.7), channel_id=1, replica_groups=mesh['sp_0'=8,'sp_1'=4,'tp'=8] {'tp'}, dimensions={1}, use_global_device_ids=true | all-gather | bytes 884736 | tf_op jit(solution)/shard_map/all_gather | solution.py:251
  153.5 1.9 all-gather.9.cloned.1.call-done
  179.0 1.6 fusion.110
  180.6 68.9 %while.45 = (s32[]{:T(128)}, f32[1,256,128]{2,1,0:T(8,128)S(1)}, f32[1,128]{1,0:T(1,128)S(1)}, f32[1]{0:T(128)}, f32[8,1,64,256]{3,2,1,0:T(8,128)S(1)}, /*index=...) while((s32[]{:T(128)}, f32[1,256,128]{2,1,0:T(8,128)S(1)}, ...), condition=%wide.region_11.12_spmd, body=%wide.region_6.11_spmd.sunk | while | flops 69588096 | bytes 982777 | solution.py:291
  249.7 13.4 %psum.7 = f32[512]{0:T(512)S(1)} all-reduce(f32[512]{0:T(512)S(1)} %reduce_sum.82), channel_id=1, replica_groups=mesh['sp_0'=8,'sp_1'=4,'tp'=8] {'tp'}, use_global_device_ids=true, to_apply=%region_13.14 | all-reduce | flops 512 | bytes 4096 | tf_op jit(solution)/shard_map/psum | solution.py:295
  263.3 2.8 fusion.176
  266.1 3.6 all-gather.7.cloned.1.call-done
  269.7 6.0 %fusion.169 = (bf16[16384,128]{0,1:T(8,128)(2,1)}, bf16[16384,128]{0,1:T(8,128)(2,1)}) fusion(bf16[16384,320]{0,1:T(8,128)(2,1)} %all-gather.7.cloned.1.call-done), kind=kLoop, calls=%fused_computation.273 | loop fusion | bytes 16777216 | tf_op jit(solution)/shard_map/split | solution.py:84
  275.7 6.4 %copy.48 = bf16[16384,128]{1,0:T(8,128)(2,1)} copy(bf16[16384,128]{0,1:T(8,128)(2,1)} %get-tuple-element.494) | data formatting | bytes 8388608 | tf_op jit(solution)/shard_map/while | solution.py:372
  282.1 1.6 slice-done
  283.7 3.1 copy.47
  286.8 6.4 %copy.45 = bf16[16384,128]{1,0:T(8,128)(2,1)} copy(bf16[16384,128]{0,1:T(8,128)(2,1)} %get-tuple-element.495) | data formatting | bytes 8388608 | tf_op jit(solution)/shard_map/while | solution.py:372
  293.2 116.5 %while.46 = (s32[]{:T(128)}, f32[1,512]{1,0:T(1,128)S(1)}, f32[1,512]{1,0:T(1,128)S(1)}, f32[1,512,128]{2,1,0:T(8,128)S(1)}, s32[16]{0:T(128)S(1)}, /*index=5*/s...) while((s32[]{:T(128)}, f32[1,512]{1,0:T(1,128)S(1)}, ...), condition=%wide.region_21.22_spmd, body=%wide.region_16.21_spmd.sunk | while | flops 340396032 | bytes 12036461 | solution.py:372
  295.7 4.9 %conditional.2 = ((f32[1,512]{1,0:T(1,128)S(1)}, f32[1,512]{1,0:T(1,128)S(1)}, f32[1,512,128]{2,1,0:T(8,128)S(1)})) conditional(s32[]{:T(128)} %convert_element_type.198, (f32[1,512]{1,0:T(1,128)S(1)}, f32[1,512]{1,0:T(1,128)S(1)}, f32[1,512,128]{2,1,0:T(8,128)S(1)}) %tuple.113, (s32[]{:T(128)}, s32[512]{0:T(512)S(1)}, ...), branch_computations={%region_17.17_spmd, %region_18.20_spmd} | conditional | flops 340396032 | bytes 12036178 | solution.py:368
  299.0 1.5 fusion.50
  302.9 4.9 %conditional.2 = ((f32[1,512]{1,0:T(1,128)S(1)}, f32[1,512]{1,0:T(1,128)S(1)}, f32[1,512,128]{2,1,0:T(8,128)S(1)})) conditional(s32[]{:T(128)} %convert_element_type.198, (f32[1,512]{1,0:T(1,128)S(1)}, f32[1,512]{1,0:T(1,128)S(1)}, f32[1,512,128]{2,1,0:T(8,128)S(1)}) %tuple.113, (s32[]{:T(128)}, s32[512]{0:T(512)S(1)}, ...), branch_computations={%region_17.17_spmd, %region_18.20_spmd} | conditional | flops 340396032 | bytes 12036178 | solution.py:368
  310.2 4.9 %conditional.2 = ((f32[1,512]{1,0:T(1,128)S(1)}, f32[1,512]{1,0:T(1,128)S(1)}, f32[1,512,128]{2,1,0:T(8,128)S(1)})) conditional(s32[]{:T(128)} %convert_element_type.198, (f32[1,512]{1,0:T(1,128)S(1)}, f32[1,512]{1,0:T(1,128)S(1)}, f32[1,512,128]{2,1,0:T(8,128)S(1)}) %tuple.113, (s32[]{:T(128)}, s32[512]{0:T(512)S(1)}, ...), branch_computations={%region_17.17_spmd, %region_18.20_spmd} | conditional | flops 340396032 | bytes 12036178 | solution.py:368
  313.6 1.5 fusion.50
  317.5 4.9 %conditional.2 = ((f32[1,512]{1,0:T(1,128)S(1)}, f32[1,512]{1,0:T(1,128)S(1)}, f32[1,512,128]{2,1,0:T(8,128)S(1)})) conditional(s32[]{:T(128)} %convert_element_type.198, (f32[1,512]{1,0:T(1,128)S(1)}, f32[1,512]{1,0:T(1,128)S(1)}, f32[1,512,128]{2,1,0:T(8,128)S(1)}) %tuple.113, (s32[]{:T(128)}, s32[512]{0:T(512)S(1)}, ...), branch_computations={%region_17.17_spmd, %region_18.20_spmd} | conditional | flops 340396032 | bytes 12036178 | solution.py:368
  324.8 4.9 %conditional.2 = ((f32[1,512]{1,0:T(1,128)S(1)}, f32[1,512]{1,0:T(1,128)S(1)}, f32[1,512,128]{2,1,0:T(8,128)S(1)})) conditional(s32[]{:T(128)} %convert_element_type.198, (f32[1,512]{1,0:T(1,128)S(1)}, f32[1,512]{1,0:T(1,128)S(1)}, f32[1,512,128]{2,1,0:T(8,128)S(1)}) %tuple.113, (s32[]{:T(128)}, s32[512]{0:T(512)S(1)}, ...), branch_computations={%region_17.17_spmd, %region_18.20_spmd} | conditional | flops 340396032 | bytes 12036178 | solution.py:368
  328.1 1.5 fusion.50
  332.1 4.9 %conditional.2 = ((f32[1,512]{1,0:T(1,128)S(1)}, f32[1,512]{1,0:T(1,128)S(1)}, f32[1,512,128]{2,1,0:T(8,128)S(1)})) conditional(s32[]{:T(128)} %convert_element_type.198, (f32[1,512]{1,0:T(1,128)S(1)}, f32[1,512]{1,0:T(1,128)S(1)}, f32[1,512,128]{2,1,0:T(8,128)S(1)}) %tuple.113, (s32[]{:T(128)}, s32[512]{0:T(512)S(1)}, ...), branch_computations={%region_17.17_spmd, %region_18.20_spmd} | conditional | flops 340396032 | bytes 12036178 | solution.py:368
  335.4 1.5 fusion.50
  339.4 4.9 %conditional.2 = ((f32[1,512]{1,0:T(1,128)S(1)}, f32[1,512]{1,0:T(1,128)S(1)}, f32[1,512,128]{2,1,0:T(8,128)S(1)})) conditional(s32[]{:T(128)} %convert_element_type.198, (f32[1,512]{1,0:T(1,128)S(1)}, f32[1,512]{1,0:T(1,128)S(1)}, f32[1,512,128]{2,1,0:T(8,128)S(1)}) %tuple.113, (s32[]{:T(128)}, s32[512]{0:T(512)S(1)}, ...), branch_computations={%region_17.17_spmd, %region_18.20_spmd} | conditional | flops 340396032 | bytes 12036178 | solution.py:368
  342.7 1.5 fusion.50
  346.7 4.9 %conditional.2 = ((f32[1,512]{1,0:T(1,128)S(1)}, f32[1,512]{1,0:T(1,128)S(1)}, f32[1,512,128]{2,1,0:T(8,128)S(1)})) conditional(s32[]{:T(128)} %convert_element_type.198, (f32[1,512]{1,0:T(1,128)S(1)}, f32[1,512]{1,0:T(1,128)S(1)}, f32[1,512,128]{2,1,0:T(8,128)S(1)}) %tuple.113, (s32[]{:T(128)}, s32[512]{0:T(512)S(1)}, ...), branch_computations={%region_17.17_spmd, %region_18.20_spmd} | conditional | flops 340396032 | bytes 12036178 | solution.py:368
  350.0 1.5 fusion.50
  353.9 4.9 %conditional.2 = ((f32[1,512]{1,0:T(1,128)S(1)}, f32[1,512]{1,0:T(1,128)S(1)}, f32[1,512,128]{2,1,0:T(8,128)S(1)})) conditional(s32[]{:T(128)} %convert_element_type.198, (f32[1,512]{1,0:T(1,128)S(1)}, f32[1,512]{1,0:T(1,128)S(1)}, f32[1,512,128]{2,1,0:T(8,128)S(1)}) %tuple.113, (s32[]{:T(128)}, s32[512]{0:T(512)S(1)}, ...), branch_computations={%region_17.17_spmd, %region_18.20_spmd} | conditional | flops 340396032 | bytes 12036178 | solution.py:368
  357.3 1.5 fusion.50
  361.2 4.9 %conditional.2 = ((f32[1,512]{1,0:T(1,128)S(1)}, f32[1,512]{1,0:T(1,128)S(1)}, f32[1,512,128]{2,1,0:T(8,128)S(1)})) conditional(s32[]{:T(128)} %convert_element_type.198, (f32[1,512]{1,0:T(1,128)S(1)}, f32[1,512]{1,0:T(1,128)S(1)}, f32[1,512,128]{2,1,0:T(8,128)S(1)}) %tuple.113, (s32[]{:T(128)}, s32[512]{0:T(512)S(1)}, ...), branch_computations={%region_17.17_spmd, %region_18.20_spmd} | conditional | flops 340396032 | bytes 12036178 | solution.py:368
  364.5 1.5 fusion.50
  368.5 4.9 %conditional.2 = ((f32[1,512]{1,0:T(1,128)S(1)}, f32[1,512]{1,0:T(1,128)S(1)}, f32[1,512,128]{2,1,0:T(8,128)S(1)})) conditional(s32[]{:T(128)} %convert_element_type.198, (f32[1,512]{1,0:T(1,128)S(1)}, f32[1,512]{1,0:T(1,128)S(1)}, f32[1,512,128]{2,1,0:T(8,128)S(1)}) %tuple.113, (s32[]{:T(128)}, s32[512]{0:T(512)S(1)}, ...), branch_computations={%region_17.17_spmd, %region_18.20_spmd} | conditional | flops 340396032 | bytes 12036178 | solution.py:368
  371.8 1.5 fusion.50
  375.8 4.9 %conditional.2 = ((f32[1,512]{1,0:T(1,128)S(1)}, f32[1,512]{1,0:T(1,128)S(1)}, f32[1,512,128]{2,1,0:T(8,128)S(1)})) conditional(s32[]{:T(128)} %convert_element_type.198, (f32[1,512]{1,0:T(1,128)S(1)}, f32[1,512]{1,0:T(1,128)S(1)}, f32[1,512,128]{2,1,0:T(8,128)S(1)}) %tuple.113, (s32[]{:T(128)}, s32[512]{0:T(512)S(1)}, ...), branch_computations={%region_17.17_spmd, %region_18.20_spmd} | conditional | flops 340396032 | bytes 12036178 | solution.py:368
  379.1 1.5 fusion.50
  383.1 4.9 %conditional.2 = ((f32[1,512]{1,0:T(1,128)S(1)}, f32[1,512]{1,0:T(1,128)S(1)}, f32[1,512,128]{2,1,0:T(8,128)S(1)})) conditional(s32[]{:T(128)} %convert_element_type.198, (f32[1,512]{1,0:T(1,128)S(1)}, f32[1,512]{1,0:T(1,128)S(1)}, f32[1,512,128]{2,1,0:T(8,128)S(1)}) %tuple.113, (s32[]{:T(128)}, s32[512]{0:T(512)S(1)}, ...), branch_computations={%region_17.17_spmd, %region_18.20_spmd} | conditional | flops 340396032 | bytes 12036178 | solution.py:368
  390.4 4.9 %conditional.2 = ((f32[1,512]{1,0:T(1,128)S(1)}, f32[1,512]{1,0:T(1,128)S(1)}, f32[1,512,128]{2,1,0:T(8,128)S(1)})) conditional(s32[]{:T(128)} %convert_element_type.198, (f32[1,512]{1,0:T(1,128)S(1)}, f32[1,512]{1,0:T(1,128)S(1)}, f32[1,512,128]{2,1,0:T(8,128)S(1)}) %tuple.113, (s32[]{:T(128)}, s32[512]{0:T(512)S(1)}, ...), branch_computations={%region_17.17_spmd, %region_18.20_spmd} | conditional | flops 340396032 | bytes 12036178 | solution.py:368
  397.6 4.9 %conditional.2 = ((f32[1,512]{1,0:T(1,128)S(1)}, f32[1,512]{1,0:T(1,128)S(1)}, f32[1,512,128]{2,1,0:T(8,128)S(1)})) conditional(s32[]{:T(128)} %convert_element_type.198, (f32[1,512]{1,0:T(1,128)S(1)}, f32[1,512]{1,0:T(1,128)S(1)}, f32[1,512,128]{2,1,0:T(8,128)S(1)}) %tuple.113, (s32[]{:T(128)}, s32[512]{0:T(512)S(1)}, ...), branch_computations={%region_17.17_spmd, %region_18.20_spmd} | conditional | flops 340396032 | bytes 12036178 | solution.py:368
  404.9 4.9 %conditional.2 = ((f32[1,512]{1,0:T(1,128)S(1)}, f32[1,512]{1,0:T(1,128)S(1)}, f32[1,512,128]{2,1,0:T(8,128)S(1)})) conditional(s32[]{:T(128)} %convert_element_type.198, (f32[1,512]{1,0:T(1,128)S(1)}, f32[1,512]{1,0:T(1,128)S(1)}, f32[1,512,128]{2,1,0:T(8,128)S(1)}) %tuple.113, (s32[]{:T(128)}, s32[512]{0:T(512)S(1)}, ...), branch_computations={%region_17.17_spmd, %region_18.20_spmd} | conditional | flops 340396032 | bytes 12036178 | solution.py:368
  409.8 3.0 add_convert_fusion
  412.8 30.7 %all_to_all.10 = bf16[8,64,2048]{2,1,0:T(8,128)(2,1)S(1)} all-to-all(bf16[8,64,2048]{2,1,0:T(8,128)(2,1)S(1)} %bitcast.447), channel_id=1, replica_groups=mesh['sp_0'=8,'sp_1'=4,'tp'=8] {'tp'}, dimensions={0} | all-to-all | bytes 4194304 | tf_op jit(solution)/shard_map/all_to_all | solution.py:95
  (412 shorter events, 193.1 us)
Async XLA Ops:
  6.5 256.8 %copy-start = (bf16[256,2048]{1,0:T(8,128)(2,1)S(1)}, bf16[256,2048]{1,0:T(8,128)(2,1)}, u32[]{:S(2)}) copy-start(bf16[256,2048]{1,0:T(8,128)(2,1)} %param.46) | copy-start | bytes 3145732
  11.1 31.6 %all-to-all-start = ((bf16[8,64,2048]{2,1,0:T(8,128)(2,1)}), bf16[8,64,2048]{2,1,0:T(8,128)(2,1)S(1)}, u32[]{:S(2)}, u32[]{:S(2)}) async-start(bf16[8,64,2048]{2,1,0:T(8,128)(2,1)} %broadcast_in_dim.36), calls=%async_computation | async-start | bytes 4194304 | tf_op jit(solution)/shard_map/all_to_all | solution.py:26
  15.6 28.7 %copy-start.10 = (f32[512,1]{0,1:T(1,128)S(1)}, f32[512,1]{0,1:T(1,128)}, u32[]{:S(2)}) copy-start(f32[512,1]{0,1:T(1,128)} %param.36) | copy-start | bytes 6148
  15.6 139.8 %all-gather.9.cloned.1.call-start = ((), (), s32[]{:S(2)}) async-start(), calls=%async_computation.3 | async-start | bytes 1216512 | tf_op jit(solution)/shard_map/all_gather | solution.py:54
  42.8 4.3 copy-start.5
  47.1 1.4 copy-start.6
  47.1 2.8 copy-start.4
  48.5 2.2 copy-start.1
  49.9 1.5 copy-start.2
  50.7 1.5 copy-start.11
  52.1 1.4 copy-start.12
  54.4 66.3 %copy-start.9 = (bf16[512,64]{0,1:T(8,128)(2,1)S(1)}, bf16[512,64]{0,1:T(8,128)(2,1)}, u32[]{:S(2)}) copy-start(bf16[512,64]{0,1:T(8,128)(2,1)} %convolution_convert_fusion.8) | copy-start | bytes 196612
  54.4 66.3 %copy-start.8 = (bf16[512,64]{0,1:T(8,128)(2,1)S(1)}, bf16[512,64]{0,1:T(8,128)(2,1)}, u32[]{:S(2)}) copy-start(bf16[512,64]{0,1:T(8,128)(2,1)} %convolution_convert_fusion.9) | copy-start | bytes 196612
  95.0 39.2 %copy-start.13 = (bf16[512,128]{1,0:T(8,128)(2,1)S(1)}, bf16[512,128]{1,0:T(8,128)(2,1)}, u32[]{:S(2)}) copy-start(bf16[512,128]{1,0:T(8,128)(2,1)} %param.45) | copy-start | bytes 393220
  95.1 39.2 %copy-start.16 = (f32[512]{0:T(512)S(1)}, f32[512]{0:T(512)}, u32[]{:S(2)}) copy-start(f32[512]{0:T(512)} %param.42) | copy-start | bytes 6148
  108.6 26.0 %copy-start.14 = (bf16[512,128]{1,0:T(8,128)(2,1)S(1)}, bf16[512,128]{1,0:T(8,128)(2,1)}, u32[]{:S(2)}) copy-start(bf16[512,128]{1,0:T(8,128)(2,1)} %param.44) | copy-start | bytes 393220
  120.5 149.1 %all-gather.7.cloned.1.call-start = ((), (), s32[]{:S(2)}) async-start(), calls=%async_computation.2 | async-start | bytes 10813440 | tf_op jit(solution)/shard_map/all_gather | solution.py:84
  134.6 17.0 %copy-start.15 = (f32[768]{0:T(1024)S(1)}, f32[768]{0:T(1024)}, u32[]{:S(2)}) copy-start(f32[768]{0:T(1024)} %param.41) | copy-start | bytes 9220
  180.6 82.6 %copy-start.7 = (bf16[512,256]{1,0:T(8,128)(2,1)S(1)}, bf16[512,256]{1,0:T(8,128)(2,1)}, u32[]{:S(2)}) copy-start(bf16[512,256]{1,0:T(8,128)(2,1)} %convolution_convert_fusion) | copy-start | bytes 786436
  282.1 1.6 slice-start
  293.2 116.6 %copy-start.3 = (bf16[128,2048]{1,0:T(8,128)(2,1)S(1)}, bf16[128,2048]{1,0:T(8,128)(2,1)}, u32[]{:S(2)}) copy-start(bf16[128,2048]{1,0:T(8,128)(2,1)} %param.47) | copy-start | bytes 1572868
Sparse Core Ops, SparseCore 0:
  120.6 34.7 all-gather.8
  157.9 111.7 all-gather.6
where the time goes:
time: 457 us; the launch traced here: 451 us
  matrix products  134 us (29%)
  blocking collectives  84.2 us (18%)
  local copies, waits for them, and re-layouts  57.2 us (13%)
  other arithmetic  51.3 us (11%)
  between operations  45.9 us (10%)
  loops' own time  41.5 us (9%)
  waiting for transfers between devices  32.6 us (7%)
    all_to_all x1, blocking collectives, sum_at_owner(): lax.all_to_all(tiles, axis, split_axis=0, concat_axis=0, tiled=True)  30.7 us
    all_to_all x1, waiting for transfers between devices, copy_for_each(): return lax.all_to_all(copies, axis, split_axis=0, concat_axis=0, tiled=True)  27.1 us
    dot_general x16, matrix products, attend_block(): jnp.einsum('hqk,khd->hqd', probs.astype(jnp.bfloat16), value_rows.reshape...  24.4 us
    dot_general x16, matrix products, attend_block(): jnp.einsum('qhd,kd->hqk', query_rot, key_rotary, preferred_element_type=j...  23.9 us
    dot_general x16, matrix products, attend_block(): jnp.einsum('qhd,khd->hqk', query_nope, key_nope.reshape(number, att_heads...  22.4 us
    another operation x1, loops' own time, per_device(): lax.scan(one_block, carried, jnp.arange(number // size, dtype=jnp.int32))  20 us
    reduce_max x16, other arithmetic, update_state(): new_max = jnp.maximum(last_total + stabilizer, jnp.max(weight_log, axis=-1))  19.6 us
    while x4, local copies, waits for them, and re-layouts, per_device(): lax.scan(one_block, carried, jnp.arange(number // size, dtype=jnp.int32))  16 us
  transfers between devices with their start and end apart: 3, of which 3 were waited for; matrix products, arithmetic and copies ran while one was open for 16% of the time, Pallas kernels for 0%

commit v1 on v0

--- a/solution.py
+++ b/solution.py
@@ -248,7 +248,9 @@
     length = projected.shape[0]
     positions = lax.axis_index(SP) * length + jnp.arange(length, dtype=jnp.int32)
     query_whole, latent_whole = (
-        lax.all_gather(query_latent, "tp", axis=1, tiled=True),
+        jnp.concatenate(
+            lax.all_to_all(jnp.stack([query_latent] * lax.axis_size("tp")), "tp", 0, 0), axis=1
+        ),
         lax.all_gather(keyval_latent, "tp", axis=1, tiled=True),
     )
     normed_query = rms_scale(query_whole, query_gain).astype(jnp.bfloat16)

time: 457 us -> 466 us (1.020)
  blocking collectives: 84.2 us -> 70.1 us
  local copies, waits for them, and re-layouts: 57.2 us -> 65.4 us
  waiting for transfers between devices: 32.6 us -> 37.9 us
    all_gather x1 -> x0, blocking collectives: 13.4 us -> none  [per_device(): lax.all_gather(query_latent, 'tp', axis=1, tiled=True)]
    all_to_all x0 -> x1, waiting for transfers between devices: none -> 10.8 us  [per_device(): lax.all_to_all(jnp.stack([query_latent] * lax.axis_size('tp')), 'tp', 0, 0)]
    squeeze x24, local copies, waits for them, and re-layouts: 0.21 us -> 5.2 us  [per_device(): lax.scan(summary_step, empty_state, (key_blocks, value_blocks, ingate_blo...]
  transfers between devices with their start and end apart: 3 -> 4, of which waited for: 3 -> 2; matrix products, arithmetic and copies ran while one was open for 16% -> 17% of each run, Pallas kernels for 0% -> 0%
where the time goes in v1:
time: 466 us; the launch traced here: 460 us
  matrix products  135 us (29%)
  blocking collectives  70.1 us (15%)
  local copies, waits for them, and re-layouts  65.4 us (14%)
  other arithmetic  53.7 us (12%)
  between operations  47.1 us (10%)
  loops' own time  43.1 us (9%)
  waiting for transfers between devices  37.9 us (8%)
  starting transfers between devices  8.1 us (2%)
    all_to_all x1, blocking collectives, sum_at_owner(): lax.all_to_all(tiles, axis, split_axis=0, concat_axis=0, tiled=True)  29.8 us
    all_to_all x1, waiting for transfers between devices, copy_for_each(): return lax.all_to_all(copies, axis, split_axis=0, concat_axis=0, tiled=True)  27.1 us
    dot_general x16, matrix products, attend_block(): jnp.einsum('hqk,khd->hqd', probs.astype(jnp.bfloat16), value_rows.reshape...  24.4 us
    dot_general x16, matrix products, attend_block(): jnp.einsum('qhd,kd->hqk', query_rot, key_rotary, preferred_element_type=j...  24 us
    dot_general x16, matrix products, attend_block(): jnp.einsum('qhd,khd->hqk', query_nope, key_nope.reshape(number, att_heads...  22.4 us
    another operation x1, loops' own time, per_device(): lax.scan(one_block, carried, jnp.arange(number // size, dtype=jnp.int32))  20.8 us
    reduce_max x16, other arithmetic, update_state(): new_max = jnp.maximum(last_total + stabilizer, jnp.max(weight_log, axis=-1))  20.3 us
    while x4, local copies, waits for them, and re-layouts, per_device(): lax.scan(one_block, carried, jnp.arange(number // size, dtype=jnp.int32))  16.1 us
  transfers between devices with their start and end apart: 4, of which 2 were waited for; matrix products, arithmetic and copies ran while one was open for 17% of the time, Pallas kernels for 0%

profile of v1, /device:TPU:230, one launch (start us, length us, event | category | flops | bytes accessed | tf_op | source)
XLA Modules:
  0.0 460.4 jit_solution(2299031717601269815)
XLA Ops:
  9.5 1.6 broadcast_in_dim.36
  11.1 4.5 all-to-all-start
  15.7 27.1 %all-to-all-done = bf16[8,64,2048]{2,1,0:T(8,128)(2,1)S(1)} async-done(((bf16[8,64,2048]{2,1,0:T(8,128)(2,1)}), bf16[8,64,2048]{2,1,0:T(8,128)(2,1)S(1)}, u32[]{:S(2)}, u32[]{:S(2)}) %all-to-all-start) | async-done | bytes 2097184 | tf_op jit(solution)/shard_map/all_to_all | solution.py:26
  44.3 2.1 negate_reduce_fusion
  55.6 43.0 %while.47 = (s32[]{:T(128)}, f32[1,256,128]{2,1,0:T(8,128)S(1)}, f32[1,128]{1,0:T(1,128)S(1)}, f32[1]{0:T(128)}, f32[8,1,64]{2,1,0:T(1,128)S(1)}, /*index=5*/f32...) while((s32[]{:T(128)}, f32[1,256,128]{2,1,0:T(8,128)S(1)}, ...), condition=%wide.region_4.5_spmd.clone, body=%wide.region_1.0_spmd.clone.sunk | while | flops 25383812 | bytes 401378 | solution.py:280
  98.7 13.5 %all-gather.2 = f32[4,259,128]{2,1,0:T(8,128)S(1)} all-gather(f32[1,259,128]{2,1,0:T(8,128)S(1)} %maximum_bitcast_fusion), channel_id=2, replica_groups=mesh['sp_0'=8,'sp_1'=4,'tp'=8] {'sp_1'}, dimensions={0}, use_global_device_ids=true | all-gather | bytes 663040 | tf_op jit(solution)/shard_map/all_gather | solution.py:54
  125.3 13.1 %all_gather.22 = bf16[512,512]{0,1:T(8,128)(2,1)S(1)} all-gather(bf16[512,64]{0,1:T(8,128)(2,1)S(1)} %copy-done.14), channel_id=1, replica_groups=mesh['sp_0'=8,'sp_1'=4,'tp'=8] {'tp'}, dimensions={1}, use_global_device_ids=true | all-gather | bytes 589824 | tf_op jit(solution)/shard_map/all_gather | solution.py:254
  141.4 3.5 all-to-all-start.1
  147.3 10.8 %all-to-all-done.1 = bf16[8,512,96]{1,2,0:T(8,128)(2,1)S(1)} async-done(((bf16[8,512,96]{1,2,0:T(8,128)(2,1)}), bf16[8,512,96]{1,2,0:T(8,128)(2,1)S(1)}, u32[]{:S(2)}, u32[]{:S(2)}) %all-to-all-start.1) | async-done | bytes 786464 | tf_op jit(solution)/shard_map/all_to_all | solution.py:252
  184.6 1.6 fusion.106
  186.3 74.6 %while.45 = (s32[]{:T(128)}, f32[1,256,128]{2,1,0:T(8,128)S(1)}, f32[1,128]{1,0:T(1,128)S(1)}, f32[1]{0:T(128)}, f32[8,1,64,256]{3,2,1,0:T(8,128)S(1)}, /*index=...) while((s32[]{:T(128)}, f32[1,256,128]{2,1,0:T(8,128)S(1)}, ...), condition=%wide.region_11.12_spmd, body=%wide.region_6.11_spmd.sunk | while | flops 69588096 | bytes 982777 | solution.py:293
  261.1 13.7 %psum.7 = f32[512]{0:T(512)S(1)} all-reduce(f32[512]{0:T(512)S(1)} %reduce_sum.82), channel_id=1, replica_groups=mesh['sp_0'=8,'sp_1'=4,'tp'=8] {'tp'}, use_global_device_ids=true, to_apply=%region_13.14 | all-reduce | flops 512 | bytes 4096 | tf_op jit(solution)/shard_map/psum | solution.py:297
  275.0 2.8 fusion.172
  277.7 6.0 %fusion.165 = (bf16[16384,128]{0,1:T(8,128)(2,1)}, bf16[16384,128]{0,1:T(8,128)(2,1)}) fusion(bf16[16384,320]{0,1:T(8,128)(2,1)} %all-gather.7.cloned.1.call-done), kind=kLoop, calls=%fused_computation.270 | loop fusion | bytes 16777216 | tf_op jit(solution)/shard_map/split | solution.py:84
  283.7 6.4 %copy.49 = bf16[16384,128]{1,0:T(8,128)(2,1)} copy(bf16[16384,128]{0,1:T(8,128)(2,1)} %get-tuple-element.494) | data formatting | bytes 8388608 | tf_op jit(solution)/shard_map/while | solution.py:374
  290.1 1.6 slice-done
  291.7 3.2 copy.48
  294.9 6.4 %copy.46 = bf16[16384,128]{1,0:T(8,128)(2,1)} copy(bf16[16384,128]{0,1:T(8,128)(2,1)} %get-tuple-element.495) | data formatting | bytes 8388608 | tf_op jit(solution)/shard_map/while | solution.py:374
  301.4 118.3 %while.46 = (s32[]{:T(128)}, f32[1,512]{1,0:T(1,128)S(1)}, f32[1,512]{1,0:T(1,128)S(1)}, f32[1,512,128]{2,1,0:T(8,128)S(1)}, s32[16]{0:T(128)S(1)}, /*index=5*/s...) while((s32[]{:T(128)}, f32[1,512]{1,0:T(1,128)S(1)}, ...), condition=%wide.region_21.22_spmd, body=%wide.region_16.21_spmd.sunk | while | flops 340396032 | bytes 12036461 | solution.py:374
  303.9 4.9 %conditional.2 = ((f32[1,512]{1,0:T(1,128)S(1)}, f32[1,512]{1,0:T(1,128)S(1)}, f32[1,512,128]{2,1,0:T(8,128)S(1)})) conditional(s32[]{:T(128)} %convert_element_type.205, (f32[1,512]{1,0:T(1,128)S(1)}, f32[1,512]{1,0:T(1,128)S(1)}, f32[1,512,128]{2,1,0:T(8,128)S(1)}) %tuple.113, (s32[]{:T(128)}, s32[512]{0:T(512)S(1)}, ...), branch_computations={%region_17.17_spmd, %region_18.20_spmd} | conditional | flops 340396032 | bytes 12036178 | solution.py:370
  307.2 1.5 fusion.50
  311.3 4.9 %conditional.2 = ((f32[1,512]{1,0:T(1,128)S(1)}, f32[1,512]{1,0:T(1,128)S(1)}, f32[1,512,128]{2,1,0:T(8,128)S(1)})) conditional(s32[]{:T(128)} %convert_element_type.205, (f32[1,512]{1,0:T(1,128)S(1)}, f32[1,512]{1,0:T(1,128)S(1)}, f32[1,512,128]{2,1,0:T(8,128)S(1)}) %tuple.113, (s32[]{:T(128)}, s32[512]{0:T(512)S(1)}, ...), branch_computations={%region_17.17_spmd, %region_18.20_spmd} | conditional | flops 340396032 | bytes 12036178 | solution.py:370
  314.6 1.5 fusion.50
  318.6 4.9 %conditional.2 = ((f32[1,512]{1,0:T(1,128)S(1)}, f32[1,512]{1,0:T(1,128)S(1)}, f32[1,512,128]{2,1,0:T(8,128)S(1)})) conditional(s32[]{:T(128)} %convert_element_type.205, (f32[1,512]{1,0:T(1,128)S(1)}, f32[1,512]{1,0:T(1,128)S(1)}, f32[1,512,128]{2,1,0:T(8,128)S(1)}) %tuple.113, (s32[]{:T(128)}, s32[512]{0:T(512)S(1)}, ...), branch_computations={%region_17.17_spmd, %region_18.20_spmd} | conditional | flops 340396032 | bytes 12036178 | solution.py:370
  322.0 1.5 fusion.50
  326.0 4.9 %conditional.2 = ((f32[1,512]{1,0:T(1,128)S(1)}, f32[1,512]{1,0:T(1,128)S(1)}, f32[1,512,128]{2,1,0:T(8,128)S(1)})) conditional(s32[]{:T(128)} %convert_element_type.205, (f32[1,512]{1,0:T(1,128)S(1)}, f32[1,512]{1,0:T(1,128)S(1)}, f32[1,512,128]{2,1,0:T(8,128)S(1)}) %tuple.113, (s32[]{:T(128)}, s32[512]{0:T(512)S(1)}, ...), branch_computations={%region_17.17_spmd, %region_18.20_spmd} | conditional | flops 340396032 | bytes 12036178 | solution.py:370
  329.4 1.5 fusion.50
  333.4 4.9 %conditional.2 = ((f32[1,512]{1,0:T(1,128)S(1)}, f32[1,512]{1,0:T(1,128)S(1)}, f32[1,512,128]{2,1,0:T(8,128)S(1)})) conditional(s32[]{:T(128)} %convert_element_type.205, (f32[1,512]{1,0:T(1,128)S(1)}, f32[1,512]{1,0:T(1,128)S(1)}, f32[1,512,128]{2,1,0:T(8,128)S(1)}) %tuple.113, (s32[]{:T(128)}, s32[512]{0:T(512)S(1)}, ...), branch_computations={%region_17.17_spmd, %region_18.20_spmd} | conditional | flops 340396032 | bytes 12036178 | solution.py:370
  336.8 1.5 fusion.50
  340.8 4.9 %conditional.2 = ((f32[1,512]{1,0:T(1,128)S(1)}, f32[1,512]{1,0:T(1,128)S(1)}, f32[1,512,128]{2,1,0:T(8,128)S(1)})) conditional(s32[]{:T(128)} %convert_element_type.205, (f32[1,512]{1,0:T(1,128)S(1)}, f32[1,512]{1,0:T(1,128)S(1)}, f32[1,512,128]{2,1,0:T(8,128)S(1)}) %tuple.113, (s32[]{:T(128)}, s32[512]{0:T(512)S(1)}, ...), branch_computations={%region_17.17_spmd, %region_18.20_spmd} | conditional | flops 340396032 | bytes 12036178 | solution.py:370
  344.2 1.5 fusion.50
  348.2 4.9 %conditional.2 = ((f32[1,512]{1,0:T(1,128)S(1)}, f32[1,512]{1,0:T(1,128)S(1)}, f32[1,512,128]{2,1,0:T(8,128)S(1)})) conditional(s32[]{:T(128)} %convert_element_type.205, (f32[1,512]{1,0:T(1,128)S(1)}, f32[1,512]{1,0:T(1,128)S(1)}, f32[1,512,128]{2,1,0:T(8,128)S(1)}) %tuple.113, (s32[]{:T(128)}, s32[512]{0:T(512)S(1)}, ...), branch_computations={%region_17.17_spmd, %region_18.20_spmd} | conditional | flops 340396032 | bytes 12036178 | solution.py:370
  351.6 1.5 fusion.50
  355.6 4.9 %conditional.2 = ((f32[1,512]{1,0:T(1,128)S(1)}, f32[1,512]{1,0:T(1,128)S(1)}, f32[1,512,128]{2,1,0:T(8,128)S(1)})) conditional(s32[]{:T(128)} %convert_element_type.205, (f32[1,512]{1,0:T(1,128)S(1)}, f32[1,512]{1,0:T(1,128)S(1)}, f32[1,512,128]{2,1,0:T(8,128)S(1)}) %tuple.113, (s32[]{:T(128)}, s32[512]{0:T(512)S(1)}, ...), branch_computations={%region_17.17_spmd, %region_18.20_spmd} | conditional | flops 340396032 | bytes 12036178 | solution.py:370
  358.9 1.5 fusion.50
  363.0 4.9 %conditional.2 = ((f32[1,512]{1,0:T(1,128)S(1)}, f32[1,512]{1,0:T(1,128)S(1)}, f32[1,512,128]{2,1,0:T(8,128)S(1)})) conditional(s32[]{:T(128)} %convert_element_type.205, (f32[1,512]{1,0:T(1,128)S(1)}, f32[1,512]{1,0:T(1,128)S(1)}, f32[1,512,128]{2,1,0:T(8,128)S(1)}) %tuple.113, (s32[]{:T(128)}, s32[512]{0:T(512)S(1)}, ...), branch_computations={%region_17.17_spmd, %region_18.20_spmd} | conditional | flops 340396032 | bytes 12036178 | solution.py:370
  370.4 4.9 %conditional.2 = ((f32[1,512]{1,0:T(1,128)S(1)}, f32[1,512]{1,0:T(1,128)S(1)}, f32[1,512,128]{2,1,0:T(8,128)S(1)})) conditional(s32[]{:T(128)} %convert_element_type.205, (f32[1,512]{1,0:T(1,128)S(1)}, f32[1,512]{1,0:T(1,128)S(1)}, f32[1,512,128]{2,1,0:T(8,128)S(1)}) %tuple.113, (s32[]{:T(128)}, s32[512]{0:T(512)S(1)}, ...), branch_computations={%region_17.17_spmd, %region_18.20_spmd} | conditional | flops 340396032 | bytes 12036178 | solution.py:370
  373.7 1.5 fusion.50
  377.8 4.9 %conditional.2 = ((f32[1,512]{1,0:T(1,128)S(1)}, f32[1,512]{1,0:T(1,128)S(1)}, f32[1,512,128]{2,1,0:T(8,128)S(1)})) conditional(s32[]{:T(128)} %convert_element_type.205, (f32[1,512]{1,0:T(1,128)S(1)}, f32[1,512]{1,0:T(1,128)S(1)}, f32[1,512,128]{2,1,0:T(8,128)S(1)}) %tuple.113, (s32[]{:T(128)}, s32[512]{0:T(512)S(1)}, ...), branch_computations={%region_17.17_spmd, %region_18.20_spmd} | conditional | flops 340396032 | bytes 12036178 | solution.py:370
  381.1 1.5 fusion.50
  385.2 4.9 %conditional.2 = ((f32[1,512]{1,0:T(1,128)S(1)}, f32[1,512]{1,0:T(1,128)S(1)}, f32[1,512,128]{2,1,0:T(8,128)S(1)})) conditional(s32[]{:T(128)} %convert_element_type.205, (f32[1,512]{1,0:T(1,128)S(1)}, f32[1,512]{1,0:T(1,128)S(1)}, f32[1,512,128]{2,1,0:T(8,128)S(1)}) %tuple.113, (s32[]{:T(128)}, s32[512]{0:T(512)S(1)}, ...), branch_computations={%region_17.17_spmd, %region_18.20_spmd} | conditional | flops 340396032 | bytes 12036178 | solution.py:370
  392.6 4.9 %conditional.2 = ((f32[1,512]{1,0:T(1,128)S(1)}, f32[1,512]{1,0:T(1,128)S(1)}, f32[1,512,128]{2,1,0:T(8,128)S(1)})) conditional(s32[]{:T(128)} %convert_element_type.205, (f32[1,512]{1,0:T(1,128)S(1)}, f32[1,512]{1,0:T(1,128)S(1)}, f32[1,512,128]{2,1,0:T(8,128)S(1)}) %tuple.113, (s32[]{:T(128)}, s32[512]{0:T(512)S(1)}, ...), branch_computations={%region_17.17_spmd, %region_18.20_spmd} | conditional | flops 340396032 | bytes 12036178 | solution.py:370
  400.0 4.9 %conditional.2 = ((f32[1,512]{1,0:T(1,128)S(1)}, f32[1,512]{1,0:T(1,128)S(1)}, f32[1,512,128]{2,1,0:T(8,128)S(1)})) conditional(s32[]{:T(128)} %convert_element_type.205, (f32[1,512]{1,0:T(1,128)S(1)}, f32[1,512]{1,0:T(1,128)S(1)}, f32[1,512,128]{2,1,0:T(8,128)S(1)}) %tuple.113, (s32[]{:T(128)}, s32[512]{0:T(512)S(1)}, ...), branch_computations={%region_17.17_spmd, %region_18.20_spmd} | conditional | flops 340396032 | bytes 12036178 | solution.py:370
  407.4 4.9 %conditional.2 = ((f32[1,512]{1,0:T(1,128)S(1)}, f32[1,512]{1,0:T(1,128)S(1)}, f32[1,512,128]{2,1,0:T(8,128)S(1)})) conditional(s32[]{:T(128)} %convert_element_type.205, (f32[1,512]{1,0:T(1,128)S(1)}, f32[1,512]{1,0:T(1,128)S(1)}, f32[1,512,128]{2,1,0:T(8,128)S(1)}) %tuple.113, (s32[]{:T(128)}, s32[512]{0:T(512)S(1)}, ...), branch_computations={%region_17.17_spmd, %region_18.20_spmd} | conditional | flops 340396032 | bytes 12036178 | solution.py:370
  414.8 4.9 %conditional.2 = ((f32[1,512]{1,0:T(1,128)S(1)}, f32[1,512]{1,0:T(1,128)S(1)}, f32[1,512,128]{2,1,0:T(8,128)S(1)})) conditional(s32[]{:T(128)} %convert_element_type.205, (f32[1,512]{1,0:T(1,128)S(1)}, f32[1,512]{1,0:T(1,128)S(1)}, f32[1,512,128]{2,1,0:T(8,128)S(1)}) %tuple.113, (s32[]{:T(128)}, s32[512]{0:T(512)S(1)}, ...), branch_computations={%region_17.17_spmd, %region_18.20_spmd} | conditional | flops 340396032 | bytes 12036178 | solution.py:370
  418.1 1.5 fusion.50
  419.7 3.0 add_convert_fusion
  422.6 29.8 %all_to_all.15 = bf16[8,64,2048]{2,1,0:T(8,128)(2,1)S(1)} all-to-all(bf16[8,64,2048]{2,1,0:T(8,128)(2,1)S(1)} %bitcast.456), channel_id=1, replica_groups=mesh['sp_0'=8,'sp_1'=4,'tp'=8] {'tp'}, dimensions={0} | all-to-all | bytes 4194304 | tf_op jit(solution)/shard_map/all_to_all | solution.py:95
  (435 shorter events, 202.9 us)
Async XLA Ops:
  6.5 268.4 %copy-start = (bf16[256,2048]{1,0:T(8,128)(2,1)S(1)}, bf16[256,2048]{1,0:T(8,128)(2,1)}, u32[]{:S(2)}) copy-start(bf16[256,2048]{1,0:T(8,128)(2,1)} %param.46) | copy-start | bytes 3145732
  11.1 31.6 %all-to-all-start = ((bf16[8,64,2048]{2,1,0:T(8,128)(2,1)}), bf16[8,64,2048]{2,1,0:T(8,128)(2,1)S(1)}, u32[]{:S(2)}, u32[]{:S(2)}) async-start(bf16[8,64,2048]{2,1,0:T(8,128)(2,1)} %broadcast_in_dim.36), calls=%async_computation | async-start | bytes 4194304 | tf_op jit(solution)/shard_map/all_to_all | solution.py:26
  15.6 28.7 %copy-start.21 = (f32[512,1]{0,1:T(1,128)S(1)}, f32[512,1]{0,1:T(1,128)}, u32[]{:S(2)}) copy-start(f32[512,1]{0,1:T(1,128)} %param.36) | copy-start | bytes 6148
  15.6 144.9 %all-gather.9.cloned.1.call-start = ((), (), s32[]{:S(2)}) async-start(), calls=%async_computation.4 | async-start | bytes 1216512 | tf_op jit(solution)/shard_map/all_gather | solution.py:54
  42.7 4.3 copy-start.11
  47.1 1.4 copy-start.12
  47.1 2.8 copy-start.9
  48.5 2.8 copy-start.4
  49.9 2.1 copy-start.5
  51.3 2.1 copy-start.22
  53.4 1.4 copy-start.23
  55.6 69.7 %copy-start.15 = (bf16[512,64]{0,1:T(8,128)(2,1)S(1)}, bf16[512,64]{0,1:T(8,128)(2,1)}, u32[]{:S(2)}) copy-start(bf16[512,64]{0,1:T(8,128)(2,1)} %convolution_convert_fusion.8) | copy-start | bytes 196612
  55.6 69.7 %copy-start.14 = (bf16[512,64]{0,1:T(8,128)(2,1)S(1)}, bf16[512,64]{0,1:T(8,128)(2,1)}, u32[]{:S(2)}) copy-start(bf16[512,64]{0,1:T(8,128)(2,1)} %convolution_convert_fusion.9) | copy-start | bytes 196612
  98.6 24.0 %copy-start.17 = (f32[8,1,64]{2,1,0:T(1,128)}, f32[8,1,64]{2,1,0:T(1,128)S(1)}, u32[]{:S(2)}) copy-start(f32[8,1,64]{2,1,0:T(1,128)S(1)} %get-tuple-element.858) | copy-start | bytes 6148
  98.7 40.3 %copy-start.24 = (bf16[512,128]{1,0:T(8,128)(2,1)S(1)}, bf16[512,128]{1,0:T(8,128)(2,1)}, u32[]{:S(2)}) copy-start(bf16[512,128]{1,0:T(8,128)(2,1)} %param.45) | copy-start | bytes 393220
  98.7 40.3 %copy-start.26 = (f32[512]{0:T(512)S(1)}, f32[512]{0:T(512)}, u32[]{:S(2)}) copy-start(f32[512]{0:T(512)} %param.42) | copy-start | bytes 6148
  112.2 27.1 %copy-start.25 = (bf16[512,128]{1,0:T(8,128)(2,1)S(1)}, bf16[512,128]{1,0:T(8,128)(2,1)}, u32[]{:S(2)}) copy-start(bf16[512,128]{1,0:T(8,128)(2,1)} %param.44) | copy-start | bytes 393220
  125.2 152.6 %all-gather.7.cloned.1.call-start = ((), (), s32[]{:S(2)}) async-start(), calls=%async_computation.3 | async-start | bytes 10813440 | tf_op jit(solution)/shard_map/all_gather | solution.py:84
  125.2 13.7 %copy-start.18 = (f32[32]{0:T(128)}, f32[32]{0:T(128)S(1)}, u32[]{:S(2)}) copy-start(f32[32]{0:T(128)S(1)} %multiply_power_fusion) | copy-start | bytes 388
  138.4 2.1 copy-start.8
  139.3 7.1 %copy-start.7 = (bf16[512,128]{1,0:T(8,128)(2,1)S(1)}, bf16[512,128]{1,0:T(8,128)(2,1)}, u32[]{:S(2)}) copy-start(bf16[512,128]{1,0:T(8,128)(2,1)} %convolution_convert_fusion.6) | copy-start | bytes 393220
  140.4 17.8 %copy-start.16 = (f32[768]{0:T(1024)S(1)}, f32[768]{0:T(1024)}, u32[]{:S(2)}) copy-start(f32[768]{0:T(1024)} %param.41) | copy-start | bytes 9220
  141.4 16.6 %all-to-all-start.1 = ((bf16[8,512,96]{1,2,0:T(8,128)(2,1)}), bf16[8,512,96]{1,2,0:T(8,128)(2,1)S(1)}, u32[]{:S(2)}, u32[]{:S(2)}) async-start(bf16[8,512,96]{1,2,0:T(8,128)(2,1)} %stack.2), calls=%async_computation.1 | async-start | bytes 1572864 | tf_op jit(solution)/shard_map/all_to_all | solution.py:252
  147.3 12.2 %copy-start.19 = (f32[32]{0:T(128)S(1)}, f32[32]{0:T(128)}, u32[]{:S(2)}) copy-start(f32[32]{0:T(128)} %copy-done.18) | copy-start | bytes 388
  158.0 1.0 copy-start.10
  158.3 25.6 %copy-start.20 = (f32[1,1,128]{2,1,0:T(1,128)S(1)}, f32[1,1,128]{2,1,0:T(1,128)}, u32[]{:S(2)}) copy-start(f32[1,1,128]{2,1,0:T(1,128)} %get-tuple-element.488) | copy-start | bytes 1540
  159.0 27.2 %copy-start.3 = (f32[8,1,64,256]{3,2,1,0:T(8,128)S(1)}, f32[8,1,64,256]{3,2,1,0:T(8,128)}, u32[]{:S(2)}) copy-start(f32[8,1,64,256]{3,2,1,0:T(8,128)} %custom-call.2) | copy-start | bytes 1572868
  186.3 88.5 %copy-start.13 = (bf16[512,256]{1,0:T(8,128)(2,1)S(1)}, bf16[512,256]{1,0:T(8,128)(2,1)}, u32[]{:S(2)}) copy-start(bf16[512,256]{1,0:T(8,128)(2,1)} %convolution_convert_fusion) | copy-start | bytes 786436
  290.1 1.6 slice-start
  294.9 6.4 %copy-start.2 = (bf16[512,1,64]{0,2,1:T(8,128)(2,1)S(1)}, bf16[512,1,64]{0,2,1:T(8,128)(2,1)}, u32[]{:S(2)}) copy-start(bf16[512,1,64]{0,2,1:T(8,128)(2,1)} %pad_maximum_fusion.1) | copy-start | bytes 196612
  301.3 118.3 %copy-start.6 = (bf16[128,2048]{1,0:T(8,128)(2,1)S(1)}, bf16[128,2048]{1,0:T(8,128)(2,1)}, u32[]{:S(2)}) copy-start(bf16[128,2048]{1,0:T(8,128)(2,1)} %param.47) | copy-start | bytes 1572868
  422.6 30.9 %copy-start.1 = (bf16[256,2048]{1,0:T(8,128)(2,1)S(1)}, bf16[256,2048]{1,0:T(8,128)(2,1)}, u32[]{:S(2)}) copy-start(bf16[256,2048]{1,0:T(8,128)(2,1)} %param.46) | copy-start | bytes 3145732
Sparse Core Ops, SparseCore 0:
  125.3 34.7 all-gather.8
  162.6 110.8 all-gather.6
